TPU v7x, 32 devices: a whole 2x2x4 slice. The times are simulated.
32 devices in a mesh: kv: 16 (over z, y, core), tp: 2 (over x).
Axes of the slice: x: 2, y: 2, z: 4, core: 2. Of those that a mesh axis runs over, the one named last changes fastest.
Arguments:
- queries: bfloat16 [4096, 4, 128], P('kv', 'tp'), may hold values from -6 to 6
- keys: bfloat16 [4096, 4, 128], P('kv', 'tp'), may hold values from -6 to 6
- values: bfloat16 [4096, 4, 128], P('kv', 'tp'), may hold values from -6 to 6
- attended: bfloat16 [4096, 4, 128], P('kv', 'tp'), may hold values from -6 to 6
- out_grad: bfloat16 [4096, 4, 128], P('kv', 'tp'), may hold values from -6 to 6
- log_sum: float32 [4096, 4], P('kv', 'tp'), may hold values from 2.5 to 4.5
- picked: int32 [32, 16], P('kv'), may hold values from -1 to 127, as said below
- layer_input: bfloat16 [4096, 4096], P('kv'), may hold values from -0.03125 to 0.03125
Outputs:
- query_grad: float32 [4096, 4, 128], P('kv', 'tp')
- key_grad: float32 [4096, 4, 128], P('kv', 'tp')
- value_grad: float32 [4096, 4, 128], P('kv', 'tp')
- weight_grad: float32 [4096, 512], P('kv', 'tp')
Inputs may be any that keep to these rules, and one draw needn't show every extreme that they name: Row r lists distinct key block numbers picked by query block r, followed by -1 to the end of the row; at least one entry is not -1, and at most 16 are. No picked block starts after the last position of its query block. With the span of a position being the position divided by 256 (rounded down), the span of every picked block is the query block's span or that span less 1, 2, 4, 8 and so on. The query blocks of one span pick at most 4 distinct blocks from any other single span.
All inputs are finite; a program needn't handle non-finite values.
Results may differ from a plain program's by a relative error of at most 0.004.
Values may be sent and summed in bfloat16 or wider, within the bound.
A program may use at most 64 MiB of HBM per device.

v0:
```python
import functools

import jax
import jax.numpy as jnp
from jax import lax
from jax.experimental import pallas as pl
from jax.experimental.pallas import tpu as pltpu
from jax.sharding import PartitionSpec as P

QB = 128
KB = 32
PER_SPAN = 4
COMPACT = PER_SPAN * KB
CHUNKS = 8
F32 = jnp.float32
BF16 = jnp.bfloat16


def xor(value, bits):
    out = value
    for i in range(bits.bit_length()):
        if bits >> i & 1:
            out = out + (1 << i) - (2 << i) * lax.rem(value // (1 << i), 2)
    return out


def dot_nt(a, b):
    return lax.dot_general(a, b, (((1,), (1,)), ((), ())), preferred_element_type=F32)


def dot_tn(a, b):
    return lax.dot_general(a, b, (((0,), (0,)), ((), ())), preferred_element_type=F32)


def dot_nn(a, b):
    return lax.dot_general(a, b, (((1,), (0,)), ((), ())), preferred_element_type=F32)


def body(
    n, levels, heads, dh,
    picked_hbm, q_hbm, k_hbm, v_hbm, att_hbm, og_hbm, log_sum, x_hbm,
    dq_out, dk_out, dv_out, wg_out,
    picked, raw, q, k, v, att, og, x, xt, slot, slot_in, pick, ksend, kin, vsend, vin, dvsend, dvin, dksend, dkin,
    wts, part, got1, send2, got2, send3, got3,
    x_sem, picked_sem, raw_sem, slot_ss, slot_rs, k_ss, k_rs, v_ss, v_rs, dv_ss, dv_rs, dk_ss, dk_rs,
    s1_ss, s1_rs, s2_ss, s2_rs, s3_ss, s3_rs,
):
    me = lax.axis_index("kv")
    tok, cols = q.shape
    query_count = tok // QB
    span_blocks = tok // KB
    rows = slot.shape[0]
    scale = dh ** (-0.5)
    quarter = n // 4
    rb = wg_out.shape[0]
    order = list(reversed(range(levels)))

    def to(offset):
        return {"kv": lax.rem(me + offset + n, n)}

    def flipped(bits):
        low = lax.rem(me, 4)
        high = me // 4
        if bits == 1:
            return {"kv": me + 1 - 2 * lax.rem(me, 2)}
        if bits == 2:
            return {"kv": me + 2 - 4 * (low // 2)}
        return {"kv": xor(high, bits // 4) * 4 + low}

    def remote(src, dst, ss, rs, device):
        return pltpu.make_async_remote_copy(
            src_ref=src, dst_ref=dst, send_sem=ss, recv_sem=rs,
            device_id=device, device_id_type=pl.DeviceIdType.MESH,
        )

    load_picked = pltpu.make_async_copy(picked_hbm, picked, picked_sem)
    load_picked.start()
    loads = {}
    for i, (src, dst) in enumerate(
        ((k_hbm, k), (v_hbm, v), (q_hbm, q), (og_hbm, og), (att_hbm, att))
    ):
        loads[i] = (pltpu.make_async_copy(src, raw.at[i], raw_sem.at[i]), dst)
        loads[i][0].start()

    def settle(i):
        copy, dst = loads[i]
        copy.wait()
        for h in range(heads):
            dst[:, h * dh : (h + 1) * dh] = raw[i, :, h, :]

    load_x = pltpu.make_async_copy(x_hbm, x, x_sem)
    load_x.start()
    barrier = pltpu.get_barrier_semaphore()
    greeted = [to(1 << l) for l in range(levels)] + [to(-(1 << l)) for l in range(levels)]
    greeted += [flipped(1), flipped(2)] + [flipped(4 * b) for b in range(1, quarter)]
    for device in greeted:
        pl.semaphore_signal(
            barrier, inc=1, device_id=device, device_id_type=pl.DeviceIdType.MESH
        )

    row = lax.broadcasted_iota(jnp.int32, (rows, tok), 0)
    lane = lax.broadcasted_iota(jnp.int32, (rows, tok), 1)
    back = jnp.zeros((rows, tok), jnp.int32)
    for l in range(levels):
        back = jnp.where(row == l + 1, 1 << l, back)
    ids = jnp.where(row <= levels, (me - back) * span_blocks + lane // KB, -2)
    load_picked.wait()
    live = []
    for b in range(query_count):
        hit = jnp.zeros((rows, tok), jnp.int32)
        for s in range(picked.shape[1]):
            p = picked[b, s]
            hit = jnp.where(ids == jnp.where(p < 0, -(1 << 30), p), 1, hit)
        live.append(hit.astype(F32))
    need = functools.reduce(jnp.maximum, live)
    below = lax.broadcasted_iota(jnp.int32, (tok, tok), 0)
    above = lax.broadcasted_iota(jnp.int32, (tok, tok), 1)
    steps = jnp.where((below % KB == 0) & (below // KB < above // KB), 1.0, 0.0).astype(BF16)
    rank = dot_nn(need.astype(BF16), steps)
    slot[...] = jnp.where(need > 0, rank * KB + (lane % KB).astype(F32), -1.0)

    settle(0)
    settle(1)
    pl.semaphore_wait(barrier, len(greeted))

    def sends_up(l):
        return me + (1 << l) < n

    def sends_down(l):
        return me >= 1 << l

    slot_copies = {}
    for l in order:
        slot_copies[l] = remote(
            slot, slot_in.at[l], slot_ss.at[l], slot_rs.at[l], to(-(1 << l))
        )
        pl.when(sends_down(l))(slot_copies[l].start)

    def one_hot(row_values):
        sub = lax.broadcasted_iota(jnp.int32, (COMPACT, tok), 0).astype(F32)
        return jnp.where(sub == row_values, 1.0, 0.0).astype(BF16)

    head = [slice(h * dh, (h + 1) * dh) for h in range(heads)]
    k_copies, v_copies, dv_copies, dk_copies = {}, {}, {}, {}
    for l in order:
        k_copies[l] = remote(ksend.at[l], kin.at[l], k_ss.at[l], k_rs.at[l], to(1 << l))
        v_copies[l] = remote(vsend.at[l], vin.at[l], v_ss.at[l], v_rs.at[l], to(1 << l))
        dv_copies[l] = remote(
            dvsend.at[l], dvin.at[l], dv_ss.at[l], dv_rs.at[l], to(-(1 << l))
        )
        dk_copies[l] = remote(
            dksend.at[l], dkin.at[l], dk_ss.at[l], dk_rs.at[l], to(-(1 << l))
        )
    for l in order:

        @pl.when(sends_up(l))
        def _(l=l):
            slot_copies[l].wait_recv()
            chosen = one_hot(slot_in[l, l + 1 : l + 2, :])
            pick[l] = chosen
            ksend[l] = dot_nn(chosen, k[...]).astype(BF16)
            k_copies[l].start()

    for l in order:

        @pl.when(sends_up(l))
        def _(l=l):
            vsend[l] = dot_nn(pick[l], v[...]).astype(BF16)
            v_copies[l].start()

    for i in range(2, 5):
        settle(i)
    dots = []
    for c in head:
        column = jnp.sum(og[:, c].astype(F32) * att[:, c].astype(F32), axis=1, keepdims=True)
        dots.append(jnp.transpose(jnp.broadcast_to(column, (tok, 128)))[0:1, :])
    stored = [log_sum[h : h + 1, :] for h in range(heads)]

    def key_mask(chosen, r):
        pieces = []
        for m in live:
            column = dot_nt(chosen, m.astype(BF16))[:, r : r + 1]
            pieces.append(jnp.broadcast_to(column, (column.shape[0], QB)))
        return jnp.concatenate(pieces, axis=1) > 0

    own_mask = key_mask(jnp.where(below == above, 1.0, 0.0).astype(BF16), 0) & (below <= above)
    for h, c in enumerate(head):
        w = jnp.where(own_mask, jnp.exp(dot_nt(k[:, c], q[:, c]) * scale - stored[h]), 0.0)
        dv_out[:, c] = dot_nn(w.astype(BF16), og[:, c])
        g = (w * (dot_nt(v[:, c], og[:, c]) - dots[h])).astype(BF16)
        dk_out[:, c] = dot_nn(g, q[:, c])
        dq_out[:, c] = dot_tn(g, k[:, c])

    masks = {
        l: key_mask(one_hot(slot[l + 1 : l + 2, :]), l + 1) for l in order
    }
    load_x.wait()
    width = x.shape[1] // CHUNKS
    for i in range(CHUNKS):
        xt[i * width : (i + 1) * width, :] = jnp.transpose(x[:, i * width : (i + 1) * width])
    for l in range(levels):

        @pl.when(sends_down(l))
        def _(l=l):
            k_copies[l].wait_recv()
            for h, c in enumerate(head):
                w = jnp.where(
                    masks[l], jnp.exp(dot_nt(kin[l, :, c], q[:, c]) * scale - stored[h]), 0.0
                )
                wts[l, h] = w
                dvsend[l, :, c] = dot_nn(w.astype(BF16), og[:, c]).astype(BF16)
            dv_copies[l].start()

    for l in range(levels):

        @pl.when(sends_down(l))
        def _(l=l):
            v_copies[l].wait_recv()
            for h, c in enumerate(head):
                g = (wts[l, h] * (dot_nt(vin[l, :, c], og[:, c]) - dots[h])).astype(BF16)
                dksend[l, :, c] = (dot_nn(g, q[:, c]) * scale).astype(BF16)
                dq_out[:, c] += dot_tn(g, kin[l, :, c])
            dk_copies[l].start()

    dq_out[...] = dq_out[...] * scale

    for l in range(levels):

        @pl.when(sends_up(l))
        def _(l=l):
            dv_copies[l].wait_recv()
            dv_out[...] += dot_tn(pick[l], dvin[l])

    rounded = dv_out[...].astype(BF16)
    core = lax.rem(me, 2)
    up = lax.rem(me, 4) // 2
    high = me // 4
    far = list(reversed(range(quarter)))
    chunk = 2 * rb
    s1, s2, s3 = [], [], []

    def share(t, at):
        first = pl.multiple_of(at * chunk, chunk)
        w = dot_nn(xt[pl.ds(first, chunk), :], rounded)
        part[t] = w.reshape(2, rb, cols)
        copy = remote(
            part.at[t, 1 - core], got1.at[t], s1_ss.at[t], s1_rs.at[t], flipped(1)
        )
        copy.start()
        s1.append(copy)

    for t, b in enumerate(far):
        share(t, 2 * xor(high, b) + 1 - up)
    for t, b in enumerate(far):
        share(quarter + t, 2 * xor(high, b) + up)
        s1[t].wait_recv()
        send2[b] = (part[t, core] + got1[t]).astype(BF16)
        copy = remote(send2.at[b], got2.at[b], s2_ss.at[b], s2_rs.at[b], flipped(2))
        copy.start()
        s2.append(copy)
    for t, b in enumerate(far):
        s1[quarter + t].wait_recv()
        kept = part[quarter + t, core] + got1[quarter + t]
        s2[t].wait_recv()
        kept = kept + got2[b].astype(F32)
        if b == 0:
            wg_out[...] = kept
        else:
            send3[b] = kept.astype(BF16)
            copy = remote(send3.at[b], got3.at[b], s3_ss.at[b], s3_rs.at[b], flipped(4 * b))
            copy.start()
            s3.append(copy)

    dk_out[...] = dk_out[...] * scale
    for l in range(levels):

        @pl.when(sends_up(l))
        def _(l=l):
            dk_copies[l].wait_recv()
            dk_out[...] += dot_tn(pick[l], dkin[l])

    for b, copy in zip(reversed(range(1, quarter)), s3):
        copy.wait_recv()
        wg_out[...] += got3[b].astype(F32)
    for l in order:
        for copies in (slot_copies, dv_copies, dk_copies):
            pl.when(sends_down(l))(copies[l].wait_send)
        for copies in (k_copies, v_copies):
            pl.when(sends_up(l))(copies[l].wait_send)
    for copy in s1 + s2 + s3:
        copy.wait_send()


def finish(dq, dk, dv, wg, dq_out, dk_out, dv_out, wg_out):
    heads, dh = dq_out.shape[1:]
    for src, dst in ((dq, dq_out), (dk, dk_out), (dv, dv_out)):
        for h in range(heads):
            dst[:, h, :] = src[:, h * dh : (h + 1) * dh]
    wg_out[...] = wg[...]


def per_device(queries, keys, values, attended, out_grad, log_sum, picked, layer_input):
    tok, heads, dh = queries.shape
    n = lax.axis_size("kv")
    levels = n.bit_length() - 1
    cols = heads * dh
    width = layer_input.shape[1]
    rb = width // n
    rows = (levels + 1 + 7) // 8 * 8
    hbm = pl.BlockSpec(memory_space=pltpu.HBM)
    vmem = pl.BlockSpec(memory_space=pltpu.VMEM)
    sems = pltpu.SemaphoreType.DMA
    level_buf = pltpu.VMEM((levels, COMPACT, cols), BF16)
    out = pl.pallas_call(
        functools.partial(body, n, levels, heads, dh),
        out_shape=[jax.ShapeDtypeStruct((tok, cols), F32)] * 3
        + [jax.ShapeDtypeStruct((rb, cols), F32)],
        in_specs=[hbm] * 6 + [vmem, hbm],
        out_specs=[vmem] * 4,
        scratch_shapes=[
            pltpu.SMEM(picked.shape, jnp.int32),
            pltpu.VMEM((5, tok, heads, dh), BF16),
        ]
        + [pltpu.VMEM((tok, cols), BF16)] * 5
        + [
            pltpu.VMEM((tok, width), BF16),
            pltpu.VMEM((width, tok), BF16),
            pltpu.VMEM((rows, tok), F32),
            pltpu.VMEM((levels, rows, tok), F32),
            pltpu.VMEM((levels, COMPACT, tok), BF16),
        ]
        + [level_buf] * 8
        + [
            pltpu.VMEM((levels, heads, COMPACT, tok), F32),
            pltpu.VMEM((n // 2, 2, rb, cols), F32),
            pltpu.VMEM((n // 2, rb, cols), F32),
            pltpu.VMEM((n // 4, rb, cols), BF16),
            pltpu.VMEM((n // 4, rb, cols), BF16),
            pltpu.VMEM((n // 4, rb, cols), BF16),
            pltpu.VMEM((n // 4, rb, cols), BF16),
            sems,
            sems,
            sems((5,)),
        ]
        + [sems((levels,))] * 10
        + [sems((n // 2,))] * 2
        + [sems((n // 4,))] * 4,
        compiler_params=pltpu.CompilerParams(
            collective_id=0, has_side_effects=True
        ),
    )(picked, queries, keys, values, attended, out_grad, log_sum.T, layer_input)
    return pl.pallas_call(
        finish,
        out_shape=[jax.ShapeDtypeStruct((tok, heads, dh), F32)] * 3
        + [jax.ShapeDtypeStruct((rb, cols), F32)],
        in_specs=[vmem] * 4,
        out_specs=[vmem] * 4,
    )(*out)


def solution(mesh):
    placed = (P("kv", "tp", None),) * 5 + (P("kv", "tp"), P("kv", None), P("kv", None))
    return jax.shard_map(
        per_device,
        mesh=mesh,
        in_specs=placed,
        out_specs=(P("kv", "tp", None), P("kv", "tp", None), P("kv", "tp", None), P("kv", "tp")),
        check_vma=False,
    )
```

profile of v0, /device:TPU:0, one launch (start us, length us, event | category | flops | bytes accessed | tf_op | source)
XLA Modules:
  0.0 49.1 jit_solution(13936607730364542260)
XLA Ops:
  0.6 46.1 %shard_map.111 = (f32[256,256]{1,0:T(8,128)}, f32[256,256]{1,0:T(8,128)}, f32[256,256]{1,0:T(8,128)}, f32[256,256]{1,0:T(8,128)}) custom-call(s32[2,16]{1,0:T(2,128)} %picked_hbm.1, bf16[256,2,128]{2,1,0:T(2,128)(2,1)} %q_hbm.1, bf16[256,2,128]{2,1,0:T(2,128)(2,1)} %k_hbm.1, bf16[256,2,128]{2,1,0:T(2,128)(2,1)} %v_hbm.1, bf16[256,2,128]{2,1,0:T(2,128)(2,1)} %att_hbm.1, ...), custom_call_target="tpu_custom_call" | custom-call | tf_op jit(solution)/shard_map/pallas_call | solution.py:314
  46.7 2.4 %shard_map.112 = (f32[256,2,128]{2,1,0:T(2,128)}, f32[256,2,128]{2,1,0:T(2,128)}, f32[256,2,128]{2,1,0:T(2,128)}, f32[256,256]{1,0:T(8,128)}) custom-call(f32[256,256]{1,0:T(8,128)} %get-tuple-element.8.dq, f32[256,256]{1,0:T(8,128)} %get-tuple-element.9.dk, f32[256,256]{1,0:T(8,128)} %get-tuple-element.10.dv, f32[256,256]{1,0:T(8,128)} %get-tuple-element.11.wg), custom_call_target="tpu_custom_call" | custom-call | tf_op jit(solution)/shard_map/pallas_call | solution.py:352
where the time goes:
time: 49.2 us; the launch traced here: 49.1 us
  Pallas kernels  48.4 us (98%)
  between operations  0.64 us (1%)
    pallas_call x1, Pallas kernels, per_device(): pl.pallas_call(functools.partial(body, n, levels, heads, dh), out_shape=[...  46.1 us
    pallas_call x1, Pallas kernels, per_device(): pl.pallas_call(finish, out_shape=[jax.ShapeDtypeStruct((tok, heads, dh),...  2.36 us

commit v1 on v0

--- a/solution.py
+++ b/solution.py
@@ -38,11 +38,11 @@
 
 def body(
     n, levels, heads, dh,
-    picked_hbm, q_hbm, k_hbm, v_hbm, att_hbm, og_hbm, log_sum, x_hbm,
+    picked_hbm, q_hbm, k_hbm, v_hbm, att_hbm, og_hbm, log_hbm, x_hbm,
     dq_out, dk_out, dv_out, wg_out,
-    picked, raw, q, k, v, att, og, x, xt, slot, slot_in, pick, ksend, kin, vsend, vin, dvsend, dvin, dksend, dkin,
+    picked, log_sum, dq, dk, dv, raw, q, k, v, att, og, x, xt, slot, slot_in, pick, ksend, kin, vsend, vin, dvsend, dvin, dksend, dkin,
     wts, part, got1, send2, got2, send3, got3,
-    x_sem, picked_sem, raw_sem, slot_ss, slot_rs, k_ss, k_rs, v_ss, v_rs, dv_ss, dv_rs, dk_ss, dk_rs,
+    x_sem, picked_sem, log_sem, raw_sem, slot_ss, slot_rs, k_ss, k_rs, v_ss, v_rs, dv_ss, dv_rs, dk_ss, dk_rs,
     s1_ss, s1_rs, s2_ss, s2_rs, s3_ss, s3_rs,
 ):
     me = lax.axis_index("kv")
@@ -75,6 +75,14 @@
 
     load_picked = pltpu.make_async_copy(picked_hbm, picked, picked_sem)
     load_picked.start()
+    barrier = pltpu.get_barrier_semaphore()
+    greeted = [to(1 << l) for l in range(levels)] + [to(-(1 << l)) for l in range(levels)]
+    greeted += [flipped(1), flipped(2)] + [flipped(4 * b) for b in range(1, quarter)]
+    for device in greeted:
+        pl.semaphore_signal(
+            barrier, inc=1, device_id=device, device_id_type=pl.DeviceIdType.MESH
+        )
+
     loads = {}
     for i, (src, dst) in enumerate(
         ((k_hbm, k), (v_hbm, v), (q_hbm, q), (og_hbm, og), (att_hbm, att))
@@ -90,14 +98,8 @@
 
     load_x = pltpu.make_async_copy(x_hbm, x, x_sem)
     load_x.start()
-    barrier = pltpu.get_barrier_semaphore()
-    greeted = [to(1 << l) for l in range(levels)] + [to(-(1 << l)) for l in range(levels)]
-    greeted += [flipped(1), flipped(2)] + [flipped(4 * b) for b in range(1, quarter)]
-    for device in greeted:
-        pl.semaphore_signal(
-            barrier, inc=1, device_id=device, device_id_type=pl.DeviceIdType.MESH
-        )
-
+    load_log = pltpu.make_async_copy(log_hbm, log_sum, log_sem)
+    load_log.start()
     row = lax.broadcasted_iota(jnp.int32, (rows, tok), 0)
     lane = lax.broadcasted_iota(jnp.int32, (rows, tok), 1)
     back = jnp.zeros((rows, tok), jnp.int32)
@@ -119,22 +121,23 @@
     rank = dot_nn(need.astype(BF16), steps)
     slot[...] = jnp.where(need > 0, rank * KB + (lane % KB).astype(F32), -1.0)
 
+    pl.semaphore_wait(barrier, len(greeted))
+
+    def sends_up(l):
+        return me + (1 << l) < n
+
+    def sends_down(l):
+        return me >= 1 << l
+
+    slot_copies = {}
+    for l in order:
+        slot_copies[l] = remote(
+            slot, slot_in.at[l], slot_ss.at[l], slot_rs.at[l], to(-(1 << l))
+        )
+        pl.when(sends_down(l))(slot_copies[l].start)
+
     settle(0)
     settle(1)
-    pl.semaphore_wait(barrier, len(greeted))
-
-    def sends_up(l):
-        return me + (1 << l) < n
-
-    def sends_down(l):
-        return me >= 1 << l
-
-    slot_copies = {}
-    for l in order:
-        slot_copies[l] = remote(
-            slot, slot_in.at[l], slot_ss.at[l], slot_rs.at[l], to(-(1 << l))
-        )
-        pl.when(sends_down(l))(slot_copies[l].start)
 
     def one_hot(row_values):
         sub = lax.broadcasted_iota(jnp.int32, (COMPACT, tok), 0).astype(F32)
@@ -174,6 +177,7 @@
     for c in head:
         column = jnp.sum(og[:, c].astype(F32) * att[:, c].astype(F32), axis=1, keepdims=True)
         dots.append(jnp.transpose(jnp.broadcast_to(column, (tok, 128)))[0:1, :])
+    load_log.wait()
     stored = [log_sum[h : h + 1, :] for h in range(heads)]
 
     def key_mask(chosen, r):
@@ -186,10 +190,10 @@
     own_mask = key_mask(jnp.where(below == above, 1.0, 0.0).astype(BF16), 0) & (below <= above)
     for h, c in enumerate(head):
         w = jnp.where(own_mask, jnp.exp(dot_nt(k[:, c], q[:, c]) * scale - stored[h]), 0.0)
-        dv_out[:, c] = dot_nn(w.astype(BF16), og[:, c])
+        dv[:, c] = dot_nn(w.astype(BF16), og[:, c])
         g = (w * (dot_nt(v[:, c], og[:, c]) - dots[h])).astype(BF16)
-        dk_out[:, c] = dot_nn(g, q[:, c])
-        dq_out[:, c] = dot_tn(g, k[:, c])
+        dk[:, c] = dot_nn(g, q[:, c])
+        dq[:, c] = dot_tn(g, k[:, c])
 
     masks = {
         l: key_mask(one_hot(slot[l + 1 : l + 2, :]), l + 1) for l in order
@@ -219,19 +223,22 @@
             for h, c in enumerate(head):
                 g = (wts[l, h] * (dot_nt(vin[l, :, c], og[:, c]) - dots[h])).astype(BF16)
                 dksend[l, :, c] = (dot_nn(g, q[:, c]) * scale).astype(BF16)
-                dq_out[:, c] += dot_tn(g, kin[l, :, c])
+                dq[:, c] += dot_tn(g, kin[l, :, c])
             dk_copies[l].start()
 
-    dq_out[...] = dq_out[...] * scale
+    def emit(src, dst, factor):
+        for h, c in enumerate(head):
+            dst[pl.ds(h, tok, stride=heads), :] = src[:, c] * factor
+
 
     for l in range(levels):
 
         @pl.when(sends_up(l))
         def _(l=l):
             dv_copies[l].wait_recv()
-            dv_out[...] += dot_tn(pick[l], dvin[l])
-
-    rounded = dv_out[...].astype(BF16)
+            dv[...] += dot_tn(pick[l], dvin[l])
+
+    rounded = dv[...].astype(BF16)
     core = lax.rem(me, 2)
     up = lax.rem(me, 4) // 2
     high = me // 4
@@ -251,6 +258,8 @@
 
     for t, b in enumerate(far):
         share(t, 2 * xor(high, b) + 1 - up)
+    emit(dq, dq_out, scale)
+    emit(dv, dv_out, 1.0)
     for t, b in enumerate(far):
         share(quarter + t, 2 * xor(high, b) + up)
         s1[t].wait_recv()
@@ -271,13 +280,15 @@
             copy.start()
             s3.append(copy)
 
-    dk_out[...] = dk_out[...] * scale
+    dk[...] = dk[...] * scale
     for l in range(levels):
 
         @pl.when(sends_up(l))
         def _(l=l):
             dk_copies[l].wait_recv()
-            dk_out[...] += dot_tn(pick[l], dkin[l])
+            dk[...] += dot_tn(pick[l], dkin[l])
+
+    emit(dk, dk_out, 1.0)
 
     for b, copy in zip(reversed(range(1, quarter)), s3):
         copy.wait_recv()
@@ -291,12 +302,15 @@
         copy.wait_send()
 
 
-def finish(dq, dk, dv, wg, dq_out, dk_out, dv_out, wg_out):
-    heads, dh = dq_out.shape[1:]
-    for src, dst in ((dq, dq_out), (dk, dk_out), (dv, dv_out)):
-        for h in range(heads):
-            dst[:, h, :] = src[:, h * dh : (h + 1) * dh]
-    wg_out[...] = wg[...]
+def finish(*refs):
+    count = len(refs) // 2
+    copies = [
+        pltpu.make_async_copy(refs[i], refs[count + i], refs[-1].at[i]) for i in range(count)
+    ]
+    for copy in copies:
+        copy.start()
+    for copy in copies:
+        copy.wait()
 
 
 def per_device(queries, keys, values, attended, out_grad, log_sum, picked, layer_input):
@@ -313,12 +327,15 @@
     level_buf = pltpu.VMEM((levels, COMPACT, cols), BF16)
     out = pl.pallas_call(
         functools.partial(body, n, levels, heads, dh),
-        out_shape=[jax.ShapeDtypeStruct((tok, cols), F32)] * 3
-        + [jax.ShapeDtypeStruct((rb, cols), F32)],
-        in_specs=[hbm] * 6 + [vmem, hbm],
+        out_shape=[pltpu.VMEM((tok * heads, dh), F32)] * 3 + [pltpu.VMEM((rb, cols), F32)],
+        in_specs=[hbm] * 8,
         out_specs=[vmem] * 4,
         scratch_shapes=[
             pltpu.SMEM(picked.shape, jnp.int32),
+            pltpu.VMEM((heads, tok), F32),
+            pltpu.VMEM((tok, cols), F32),
+            pltpu.VMEM((tok, cols), F32),
+            pltpu.VMEM((tok, cols), F32),
             pltpu.VMEM((5, tok, heads, dh), BF16),
         ]
         + [pltpu.VMEM((tok, cols), BF16)] * 5
@@ -340,6 +357,7 @@
             pltpu.VMEM((n // 4, rb, cols), BF16),
             sems,
             sems,
+            sems,
             sems((5,)),
         ]
         + [sems((levels,))] * 10
@@ -349,13 +367,14 @@
             collective_id=0, has_side_effects=True
         ),
     )(picked, queries, keys, values, attended, out_grad, log_sum.T, layer_input)
-    return pl.pallas_call(
+    dq, dk, dv, wg = pl.pallas_call(
         finish,
-        out_shape=[jax.ShapeDtypeStruct((tok, heads, dh), F32)] * 3
-        + [jax.ShapeDtypeStruct((rb, cols), F32)],
+        out_shape=[jax.ShapeDtypeStruct(o.shape, F32) for o in out],
         in_specs=[vmem] * 4,
-        out_specs=[vmem] * 4,
-    )(*out)
+        out_specs=[hbm] * 4,
+        scratch_shapes=[sems((4,))],
+    )(*(pltpu.with_memory_space_constraint(o, pltpu.VMEM) for o in out))
+    return *(g.reshape(tok, heads, dh) for g in (dq, dk, dv)), wg
 
 
 def solution(mesh):

time: 49.2 us -> 44.3 us (0.900)
  Pallas kernels: 48.4 us -> 43.4 us
    pallas_call x1, Pallas kernels: 46.1 us -> 42.4 us  [per_device(): pl.pallas_call(functools.partial(body, n, levels, heads, dh), out_shape=[...]
    pallas_call x1, Pallas kernels: 2.36 us -> 1 us  [per_device(): pl.pallas_call(finish, out_shape=[jax.ShapeDtypeStruct(o.shape, F32) for...]
where the time goes in v1:
time: 44.3 us; the launch traced here: 44.1 us
  Pallas kernels  43.4 us (98%)
  between operations  0.64 us (1%)
    pallas_call x1, Pallas kernels, per_device(): pl.pallas_call(functools.partial(body, n, levels, heads, dh), out_shape=[...  42.4 us
    pallas_call x1, Pallas kernels, per_device(): pl.pallas_call(finish, out_shape=[jax.ShapeDtypeStruct(o.shape, F32) for...  1 us

profile of v1, /device:TPU:0, one launch (start us, length us, event | category | flops | bytes accessed | tf_op | source)
XLA Modules:
  0.0 44.1 jit_solution(7607267235439607286)
XLA Ops:
  0.6 42.4 %shard_map.111 = (f32[512,128]{1,0:T(8,128)S(1)}, f32[512,128]{1,0:T(8,128)S(1)}, f32[512,128]{1,0:T(8,128)S(1)}, f32[256,256]{1,0:T(8,128)S(1)}) custom-call(s32[2,16]{1,0:T(2,128)} %picked_hbm.1, bf16[256,2,128]{2,1,0:T(2,128)(2,1)} %q_hbm.1, bf16[256,2,128]{2,1,0:T(2,128)(2,1)} %k_hbm.1, bf16[256,2,128]{2,1,0:T(2,128)(2,1)} %v_hbm.1, ...), custom_call_target="tpu_custom_call" | custom-call | tf_op jit(solution)/shard_map/pallas_call | solution.py:328
  43.1 1.0 %shard_map.112 = (f32[512,128]{1,0:T(8,128)}, f32[512,128]{1,0:T(8,128)}, f32[512,128]{1,0:T(8,128)}, f32[256,256]{1,0:T(8,128)}) custom-call(f32[512,128]{1,0:T(8,128)S(1)} %get-tuple-element.12.refs_0_, f32[512,128]{1,0:T(8,128)S(1)} %get-tuple-element.13.refs_1_, f32[512,128]{1,0:T(8,128)S(1)} %get-tuple-element.14.refs_2_, ...), custom_call_target="tpu_custom_call" | custom-call | tf_op jit(solution)/shard_map/pallas_call | solution.py:370

commit v2 on v1

--- a/solution.py
+++ b/solution.py
@@ -40,10 +40,10 @@
     n, levels, heads, dh,
     picked_hbm, q_hbm, k_hbm, v_hbm, att_hbm, og_hbm, log_hbm, x_hbm,
     dq_out, dk_out, dv_out, wg_out,
-    picked, log_sum, dq, dk, dv, raw, q, k, v, att, og, x, xt, slot, slot_in, pick, ksend, kin, vsend, vin, dvsend, dvin, dksend, dkin,
-    wts, part, got1, send2, got2, send3, got3,
+    picked, log_sum, dq, dk, dv, wg, raw, q, k, v, att, og, x, xt, slot, slot_in, pick, ksend, kin, vsend, vin, dvsend, dvin, dksend, dkin,
+    wts, part, got1, send2, got2, psend, pgot, asend, agot, bsend, bgot,
     x_sem, picked_sem, log_sem, raw_sem, slot_ss, slot_rs, k_ss, k_rs, v_ss, v_rs, dv_ss, dv_rs, dk_ss, dk_rs,
-    s1_ss, s1_rs, s2_ss, s2_rs, s3_ss, s3_rs,
+    s1_ss, s1_rs, s2_ss, s2_rs, p_ss, p_rs, a_ss, a_rs, b_ss, b_rs,
 ):
     me = lax.axis_index("kv")
     tok, cols = q.shape
@@ -53,19 +53,21 @@
     scale = dh ** (-0.5)
     quarter = n // 4
     rb = wg_out.shape[0]
+    top = levels - 1
     order = list(reversed(range(levels)))
+    landing = order
 
     def to(offset):
         return {"kv": lax.rem(me + offset + n, n)}
 
     def flipped(bits):
         low = lax.rem(me, 4)
-        high = me // 4
         if bits == 1:
             return {"kv": me + 1 - 2 * lax.rem(me, 2)}
-        if bits == 2:
-            return {"kv": me + 2 - 4 * (low // 2)}
-        return {"kv": xor(high, bits // 4) * 4 + low}
+        return {"kv": me + 2 - 4 * (low // 2)}
+
+    def tower(at):
+        return {"kv": at * 4 + lax.rem(me, 4)}
 
     def remote(src, dst, ss, rs, device):
         return pltpu.make_async_remote_copy(
@@ -77,7 +79,9 @@
     load_picked.start()
     barrier = pltpu.get_barrier_semaphore()
     greeted = [to(1 << l) for l in range(levels)] + [to(-(1 << l)) for l in range(levels)]
-    greeted += [flipped(1), flipped(2)] + [flipped(4 * b) for b in range(1, quarter)]
+    high = me // 4
+    greeted += [flipped(1), flipped(2)]
+    greeted += [tower(lax.rem(high + b, quarter)) for b in range(1, quarter)]
     for device in greeted:
         pl.semaphore_signal(
             barrier, inc=1, device_id=device, device_id_type=pl.DeviceIdType.MESH
@@ -136,6 +140,9 @@
         )
         pl.when(sends_down(l))(slot_copies[l].start)
 
+    k_copies, v_copies, dv_copies, dk_copies = {}, {}, {}, {}
+    for l in order:
+        k_copies[l] = remote(ksend.at[l], kin.at[l], k_ss.at[l], k_rs.at[l], to(1 << l))
     settle(0)
     settle(1)
 
@@ -144,9 +151,7 @@
         return jnp.where(sub == row_values, 1.0, 0.0).astype(BF16)
 
     head = [slice(h * dh, (h + 1) * dh) for h in range(heads)]
-    k_copies, v_copies, dv_copies, dk_copies = {}, {}, {}, {}
     for l in order:
-        k_copies[l] = remote(ksend.at[l], kin.at[l], k_ss.at[l], k_rs.at[l], to(1 << l))
         v_copies[l] = remote(vsend.at[l], vin.at[l], v_ss.at[l], v_rs.at[l], to(1 << l))
         dv_copies[l] = remote(
             dvsend.at[l], dvin.at[l], dv_ss.at[l], dv_rs.at[l], to(-(1 << l))
@@ -164,13 +169,18 @@
             ksend[l] = dot_nn(chosen, k[...]).astype(BF16)
             k_copies[l].start()
 
-    for l in order:
-
-        @pl.when(sends_up(l))
-        def _(l=l):
+    spot = lax.rem(me, 4)
+    near = [spot >= 1 << l for l in range(2)]
+    inside = [spot + (1 << l) < 4 for l in range(2)]
+
+    def offer(l, ready):
+        @pl.when(jnp.logical_and(sends_up(l), ready))
+        def _():
             vsend[l] = dot_nn(pick[l], v[...]).astype(BF16)
             v_copies[l].start()
 
+    for l in range(2):
+        offer(l, inside[l])
     for i in range(2, 5):
         settle(i)
     dots = []
@@ -195,17 +205,14 @@
         dk[:, c] = dot_nn(g, q[:, c])
         dq[:, c] = dot_tn(g, k[:, c])
 
-    masks = {
-        l: key_mask(one_hot(slot[l + 1 : l + 2, :]), l + 1) for l in order
-    }
+    masks = {l: key_mask(one_hot(slot[l + 1 : l + 2, :]), l + 1) for l in order}
     load_x.wait()
     width = x.shape[1] // CHUNKS
     for i in range(CHUNKS):
         xt[i * width : (i + 1) * width, :] = jnp.transpose(x[:, i * width : (i + 1) * width])
-    for l in range(levels):
-
-        @pl.when(sends_down(l))
-        def _(l=l):
+    def meet(l, ready):
+        @pl.when(jnp.logical_and(sends_down(l), ready))
+        def _():
             k_copies[l].wait_recv()
             for h, c in enumerate(head):
                 w = jnp.where(
@@ -215,10 +222,20 @@
                 dvsend[l, :, c] = dot_nn(w.astype(BF16), og[:, c]).astype(BF16)
             dv_copies[l].start()
 
-    for l in range(levels):
-
-        @pl.when(sends_down(l))
-        def _(l=l):
+    def emit(src, dst, factor):
+        for h, c in enumerate(head):
+            dst[pl.ds(h, tok, stride=heads), :] = src[:, c] * factor
+
+    for l in range(2):
+        meet(l, near[l])
+    for l in order[: levels - 2]:
+        meet(l, True)
+    for l in (1, 0):
+        meet(l, jnp.logical_not(near[l]))
+
+    def finish_level(l, ready):
+        @pl.when(jnp.logical_and(sends_down(l), ready))
+        def _():
             v_copies[l].wait_recv()
             for h, c in enumerate(head):
                 g = (wts[l, h] * (dot_nt(vin[l, :, c], og[:, c]) - dots[h])).astype(BF16)
@@ -226,12 +243,11 @@
                 dq[:, c] += dot_tn(g, kin[l, :, c])
             dk_copies[l].start()
 
-    def emit(src, dst, factor):
-        for h, c in enumerate(head):
-            dst[pl.ds(h, tok, stride=heads), :] = src[:, c] * factor
-
-
-    for l in range(levels):
+    for l in order:
+        offer(l, jnp.logical_not(inside[l]) if l < 2 else True)
+    for l in (1, 0):
+        finish_level(l, near[l])
+    for l in landing:
 
         @pl.when(sends_up(l))
         def _(l=l):
@@ -241,45 +257,143 @@
     rounded = dv[...].astype(BF16)
     core = lax.rem(me, 2)
     up = lax.rem(me, 4) // 2
-    high = me // 4
-    far = list(reversed(range(quarter)))
+    odd = lax.rem(high, 2)
+    pair = high // 2
+    pairs = quarter // 2
+    mate = 2 * pair + 1 - odd
     chunk = 2 * rb
-    s1, s2, s3 = [], [], []
-
-    def share(t, at):
-        first = pl.multiple_of(at * chunk, chunk)
+    hr = rb // 2
+    others = quarter - 2
+    turns, passes = [], []
+    for t in range(others):
+        there = lax.rem(pair + pairs - t // 2 - 1, pairs)
+        above = jnp.where(there > pair, 1, 0)
+        turns.append(2 * there + (t % 2) * (1 - above) + (1 - t % 2) * above)
+        passes.append(above != odd)
+    def arrival(landed, sem, at, h):
+        return remote(landed.at[at, h], landed.at[at, h], sem.at[at, h], sem.at[at, h], flipped(1))
+
+    s1, s2, p_copies, a_copies, b_copies = {}, {}, {}, {}, {}
+
+    def share(t, at, side):
+        first = pl.multiple_of((2 * at + side) * chunk, chunk)
         w = dot_nn(xt[pl.ds(first, chunk), :], rounded)
         part[t] = w.reshape(2, rb, cols)
-        copy = remote(
+        s1[t] = remote(
             part.at[t, 1 - core], got1.at[t], s1_ss.at[t], s1_rs.at[t], flipped(1)
         )
-        copy.start()
-        s1.append(copy)
-
-    for t, b in enumerate(far):
-        share(t, 2 * xor(high, b) + 1 - up)
+        s1[t].start()
+
+    def halves():
+        return [(h, slice(h * hr, (h + 1) * hr)) for h in range(2)]
+
+    for t in range(quarter):
+        for h in range(2):
+            s2[t, h] = remote(
+                send2.at[t, h], got2.at[t, h], s2_ss.at[t, h], s2_rs.at[t, h], flipped(2)
+            )
+    for i in range(2):
+        p_copies[i] = remote(psend.at[i], pgot.at[i], p_ss.at[i], p_rs.at[i], tower(mate))
+
+    def cross(t, extra=None):
+        s1[t].wait_recv()
+        for h, span in halves():
+            total = part[t, core, span, :] + got1[t, span, :]
+            if extra is not None:
+                total = total + extra[span, :].astype(F32)
+            send2[t, h] = total.astype(BF16)
+            s2[t, h].start()
+
+    def pack(i, t):
+        s1[t].wait_recv()
+        psend[i] = (part[t, core] + got1[t]).astype(BF16)
+
+    def relay(t):
+        at = turns[t]
+        s1[quarter + t].wait_recv()
+        for h, span in halves():
+            s2[t, h].wait_recv()
+            kept = part[quarter + t, core, span, :] + got1[quarter + t, span, :]
+            kept = kept + got2[t, h].astype(F32)
+            a_copies[t, h] = remote(
+                asend.at[t, h], agot.at[at, h], a_ss.at[t, h], a_rs.at[at, h], tower(mate)
+            )
+            b_copies[t, h] = remote(
+                bsend.at[t, h], bgot.at[high, h], b_ss.at[t, h], b_rs.at[high, h], tower(at)
+            )
+
+            @pl.when(passes[t])
+            def _(kept=kept):
+                asend[t, h] = kept.astype(BF16)
+                a_copies[t, h].start()
+
+            @pl.when(jnp.logical_not(passes[t]))
+            def _(kept=kept):
+                arrival(agot, a_rs, at, h).wait_recv()
+                bsend[t, h] = (kept + agot[at, h].astype(F32)).astype(BF16)
+                b_copies[t, h].start()
+
+    far, home = quarter - 1, 2 * quarter - 1
+    sender = passes[0]
+    joiner = jnp.logical_not(sender)
+    eager = jnp.logical_and(joiner, odd == 1)
+    patient = jnp.logical_and(joiner, odd == 0)
+    out_copies = {
+        h: remote(
+            bsend.at[others, h], bgot.at[high, h],
+            b_ss.at[others, h], b_rs.at[high, h], tower(mate),
+        )
+        for h in range(2)
+    }
+
+    def mate_out():
+        s1[home - 1].wait_recv()
+        for h, span in halves():
+            s2[others, h].wait_recv()
+            kept = part[home - 1, core, span, :] + got1[home - 1, span, :]
+            bsend[others, h] = (kept + got2[others, h].astype(F32)).astype(BF16)
+            out_copies[h].start()
+
+    share(0, turns[0], 1 - up)
+    share(others, mate, 1 - up)
+    share(home - 1, mate, up)
+    for t in range(1, others):
+        share(t, turns[t], 1 - up)
+    pl.when(eager)(lambda: cross(others))
+    cross(0)
+
+    @pl.when(sender)
+    def _():
+        pack(0, others)
+        p_copies[0].start()
+        pack(1, home - 1)
+
+    for t in range(1, others):
+        cross(t)
+    pl.when(patient)(lambda: cross(others))
+    for l in landing:
+        finish_level(l, jnp.logical_and(joiner, jnp.logical_not(near[l])) if l < 2 else joiner)
+    share(far, high, 1 - up)
+    for t in range(others):
+        share(quarter + t, turns[t], up)
+    share(home, high, up)
+    pl.when(eager)(mate_out)
+    relay(0)
+    pl.when(sender)(lambda: cross(far))
+
+    @pl.when(joiner)
+    def _():
+        p_copies[0].wait_recv()
+        cross(far, pgot.at[0])
+
+    pl.when(patient)(mate_out)
+    for t in range(1, others):
+        relay(t)
+    for l in landing:
+        finish_level(l, jnp.logical_and(sender, jnp.logical_not(near[l])) if l < 2 else sender)
+    pl.when(sender)(p_copies[1].start)
     emit(dq, dq_out, scale)
     emit(dv, dv_out, 1.0)
-    for t, b in enumerate(far):
-        share(quarter + t, 2 * xor(high, b) + up)
-        s1[t].wait_recv()
-        send2[b] = (part[t, core] + got1[t]).astype(BF16)
-        copy = remote(send2.at[b], got2.at[b], s2_ss.at[b], s2_rs.at[b], flipped(2))
-        copy.start()
-        s2.append(copy)
-    for t, b in enumerate(far):
-        s1[quarter + t].wait_recv()
-        kept = part[quarter + t, core] + got1[quarter + t]
-        s2[t].wait_recv()
-        kept = kept + got2[b].astype(F32)
-        if b == 0:
-            wg_out[...] = kept
-        else:
-            send3[b] = kept.astype(BF16)
-            copy = remote(send3.at[b], got3.at[b], s3_ss.at[b], s3_rs.at[b], flipped(4 * b))
-            copy.start()
-            s3.append(copy)
-
     dk[...] = dk[...] * scale
     for l in range(levels):
 
@@ -290,16 +404,46 @@
 
     emit(dk, dk_out, 1.0)
 
-    for b, copy in zip(reversed(range(1, quarter)), s3):
-        copy.wait_recv()
-        wg_out[...] += got3[b].astype(F32)
+    s1[home].wait_recv()
+    for h, span in halves():
+        s2[far, h].wait_recv()
+        total = part[home, core, span, :] + got1[home, span, :]
+        wg[span, :] = total + got2[far, h].astype(F32)
+
+    @pl.when(joiner)
+    def _():
+        p_copies[1].wait_recv()
+        wg[...] += pgot[1].astype(F32)
+
+    for src in range(quarter):
+        relays = jnp.where(src < high, src % 2, 1 - src % 2) == 1
+        relays = jnp.where(src == mate, passes[0], relays)
+
+        @pl.when(jnp.logical_and(src != high, relays))
+        def _(src=src):
+            for h, span in halves():
+                arrival(bgot, b_rs, src, h).wait_recv()
+                wg[span, :] += bgot[src, h].astype(F32)
+
+    wg_out[...] = wg[...]
     for l in order:
         for copies in (slot_copies, dv_copies, dk_copies):
             pl.when(sends_down(l))(copies[l].wait_send)
         for copies in (k_copies, v_copies):
             pl.when(sends_up(l))(copies[l].wait_send)
-    for copy in s1 + s2 + s3:
+    for copy in s1.values():
         copy.wait_send()
+    for (t, h), copy in s2.items():
+        if t == others:
+            pl.when(joiner)(copy.wait_send)
+        else:
+            copy.wait_send()
+    for i in range(2):
+        pl.when(sender)(p_copies[i].wait_send)
+        pl.when(joiner)(out_copies[i].wait_send)
+    for (t, h), copy in a_copies.items():
+        pl.when(passes[t])(copy.wait_send)
+        pl.when(jnp.logical_not(passes[t]))(b_copies[t, h].wait_send)
 
 
 def finish(*refs):
@@ -316,6 +460,7 @@
 def per_device(queries, keys, values, attended, out_grad, log_sum, picked, layer_input):
     tok, heads, dh = queries.shape
     n = lax.axis_size("kv")
+    quarter = n // 4
     levels = n.bit_length() - 1
     cols = heads * dh
     width = layer_input.shape[1]
@@ -336,6 +481,7 @@
             pltpu.VMEM((tok, cols), F32),
             pltpu.VMEM((tok, cols), F32),
             pltpu.VMEM((tok, cols), F32),
+            pltpu.VMEM((rb, cols), F32),
             pltpu.VMEM((5, tok, heads, dh), BF16),
         ]
         + [pltpu.VMEM((tok, cols), BF16)] * 5
@@ -351,10 +497,13 @@
             pltpu.VMEM((levels, heads, COMPACT, tok), F32),
             pltpu.VMEM((n // 2, 2, rb, cols), F32),
             pltpu.VMEM((n // 2, rb, cols), F32),
-            pltpu.VMEM((n // 4, rb, cols), BF16),
-            pltpu.VMEM((n // 4, rb, cols), BF16),
-            pltpu.VMEM((n // 4, rb, cols), BF16),
-            pltpu.VMEM((n // 4, rb, cols), BF16),
+            pltpu.VMEM((quarter, 2, rb // 2, cols), BF16),
+            pltpu.VMEM((quarter, 2, rb // 2, cols), BF16),
+            pltpu.VMEM((2, rb, cols), BF16),
+            pltpu.VMEM((2, rb, cols), BF16),
+        ]
+        + [pltpu.VMEM((quarter, 2, rb // 2, cols), BF16)] * 4
+        + [
             sems,
             sems,
             sems,
@@ -362,7 +511,9 @@
         ]
         + [sems((levels,))] * 10
         + [sems((n // 2,))] * 2
-        + [sems((n // 4,))] * 4,
+        + [sems((quarter, 2))] * 2
+        + [sems((2,))] * 2
+        + [sems((quarter, 2))] * 4,
         compiler_params=pltpu.CompilerParams(
             collective_id=0, has_side_effects=True
         ),

time: 44.3 us -> 37.7 us (0.85)
  the two profiles are of different devices: /device:TPU:0 before, /device:TPU:18 now
where the time goes in v2:
time: 37.7 us; the launch traced here: 37.6 us
  Pallas kernels  36.9 us (98%)
  between operations  0.64 us (2%)
    pallas_call x1, Pallas kernels, per_device(): pl.pallas_call(functools.partial(body, n, levels, heads, dh), out_shape=[...  35.9 us
    pallas_call x1, Pallas kernels, per_device(): pl.pallas_call(finish, out_shape=[jax.ShapeDtypeStruct(o.shape, F32) for...  1 us

profile of v2, /device:TPU:18, one launch (start us, length us, event | category | flops | bytes accessed | tf_op | source)
XLA Modules:
  0.0 37.6 jit_solution(1048182812210719074)
XLA Ops:
  0.6 35.9 %shard_map.111 = (f32[512,128]{1,0:T(8,128)S(1)}, f32[512,128]{1,0:T(8,128)S(1)}, f32[512,128]{1,0:T(8,128)S(1)}, f32[256,256]{1,0:T(8,128)S(1)}) custom-call(s32[2,16]{1,0:T(2,128)} %picked_hbm.1, bf16[256,2,128]{2,1,0:T(2,128)(2,1)} %q_hbm.1, bf16[256,2,128]{2,1,0:T(2,128)(2,1)} %k_hbm.1, bf16[256,2,128]{2,1,0:T(2,128)(2,1)} %v_hbm.1, ...), custom_call_target="tpu_custom_call" | custom-call | tf_op jit(solution)/shard_map/pallas_call | solution.py:473
  36.6 1.0 %shard_map.112 = (f32[512,128]{1,0:T(8,128)}, f32[512,128]{1,0:T(8,128)}, f32[512,128]{1,0:T(8,128)}, f32[256,256]{1,0:T(8,128)}) custom-call(f32[512,128]{1,0:T(8,128)S(1)} %get-tuple-element.12.refs_0_, f32[512,128]{1,0:T(8,128)S(1)} %get-tuple-element.13.refs_1_, f32[512,128]{1,0:T(8,128)S(1)} %get-tuple-element.14.refs_2_, ...), custom_call_target="tpu_custom_call" | custom-call | tf_op jit(solution)/shard_map/pallas_call | solution.py:521

commit v3 on v2

--- a/solution.py
+++ b/solution.py
@@ -12,6 +12,7 @@
 PER_SPAN = 4
 COMPACT = PER_SPAN * KB
 CHUNKS = 8
+PIECES = 4
 F32 = jnp.float32
 BF16 = jnp.bfloat16
 
@@ -40,10 +41,10 @@
     n, levels, heads, dh,
     picked_hbm, q_hbm, k_hbm, v_hbm, att_hbm, og_hbm, log_hbm, x_hbm,
     dq_out, dk_out, dv_out, wg_out,
-    picked, log_sum, dq, dk, dv, wg, raw, q, k, v, att, og, x, xt, slot, slot_in, pick, ksend, kin, vsend, vin, dvsend, dvin, dksend, dkin,
-    wts, part, got1, send2, got2, psend, pgot, asend, agot, bsend, bgot,
-    x_sem, picked_sem, log_sem, raw_sem, slot_ss, slot_rs, k_ss, k_rs, v_ss, v_rs, dv_ss, dv_rs, dk_ss, dk_rs,
-    s1_ss, s1_rs, s2_ss, s2_rs, p_ss, p_rs, a_ss, a_rs, b_ss, b_rs,
+    picked, log_sum, dq, dk, dv, wg, raw, q, k, v, att, og, x, xt, slot, slot_in, pick, kvsend, kin, vin, dsend, dvin, dkin,
+    wts, part, got1, send2, got2, psend, pgot, zsend, agot, bgot,
+    x_sem, picked_sem, log_sem, raw_sem, up_ss, down_ss, slot_rs, k_rs, v_rs, dv_rs, dk_rs,
+    s1_ss, s1_rs, s2_ss, s2_rs, p_ss, p_rs, z_ss, a_rs, b_rs,
 ):
     me = lax.axis_index("kv")
     tok, cols = q.shape
@@ -136,13 +137,15 @@
     slot_copies = {}
     for l in order:
         slot_copies[l] = remote(
-            slot, slot_in.at[l], slot_ss.at[l], slot_rs.at[l], to(-(1 << l))
+            slot, slot_in.at[l], down_ss.at[l], slot_rs.at[l], to(-(1 << l))
         )
         pl.when(sends_down(l))(slot_copies[l].start)
 
     k_copies, v_copies, dv_copies, dk_copies = {}, {}, {}, {}
     for l in order:
-        k_copies[l] = remote(ksend.at[l], kin.at[l], k_ss.at[l], k_rs.at[l], to(1 << l))
+        k_copies[l] = remote(
+            kvsend.at[l, 0], kin.at[l], up_ss.at[l], k_rs.at[l], to(1 << l)
+        )
     settle(0)
     settle(1)
 
@@ -152,22 +155,26 @@
 
     head = [slice(h * dh, (h + 1) * dh) for h in range(heads)]
     for l in order:
-        v_copies[l] = remote(vsend.at[l], vin.at[l], v_ss.at[l], v_rs.at[l], to(1 << l))
+        v_copies[l] = remote(
+            kvsend.at[l, 1], vin.at[l], up_ss.at[l], v_rs.at[l], to(1 << l)
+        )
         dv_copies[l] = remote(
-            dvsend.at[l], dvin.at[l], dv_ss.at[l], dv_rs.at[l], to(-(1 << l))
+            dsend.at[l, :COMPACT], dvin.at[l], down_ss.at[l], dv_rs.at[l], to(-(1 << l))
         )
         dk_copies[l] = remote(
-            dksend.at[l], dkin.at[l], dk_ss.at[l], dk_rs.at[l], to(-(1 << l))
-        )
-    for l in order:
+            dsend.at[l, COMPACT : 2 * COMPACT], dkin.at[l], down_ss.at[l], dk_rs.at[l],
+            to(-(1 << l)),
+        )
+    for l in order[: levels - 2] + [0, 1]:
 
         @pl.when(sends_up(l))
         def _(l=l):
             slot_copies[l].wait_recv()
             chosen = one_hot(slot_in[l, l + 1 : l + 2, :])
-            pick[l] = chosen
-            ksend[l] = dot_nn(chosen, k[...]).astype(BF16)
+            kvsend[l, 0] = dot_nn(chosen, k[...]).astype(BF16)
             k_copies[l].start()
+            pick[l] = jnp.transpose(chosen)
+            kvsend[l, 1] = dot_nn(chosen, v[...]).astype(BF16)
 
     spot = lax.rem(me, 4)
     near = [spot >= 1 << l for l in range(2)]
@@ -176,7 +183,6 @@
     def offer(l, ready):
         @pl.when(jnp.logical_and(sends_up(l), ready))
         def _():
-            vsend[l] = dot_nn(pick[l], v[...]).astype(BF16)
             v_copies[l].start()
 
     for l in range(2):
@@ -219,7 +225,7 @@
                     masks[l], jnp.exp(dot_nt(kin[l, :, c], q[:, c]) * scale - stored[h]), 0.0
                 )
                 wts[l, h] = w
-                dvsend[l, :, c] = dot_nn(w.astype(BF16), og[:, c]).astype(BF16)
+                dsend[l, :COMPACT, c] = dot_nn(w.astype(BF16), og[:, c]).astype(BF16)
             dv_copies[l].start()
 
     def emit(src, dst, factor):
@@ -239,7 +245,7 @@
             v_copies[l].wait_recv()
             for h, c in enumerate(head):
                 g = (wts[l, h] * (dot_nt(vin[l, :, c], og[:, c]) - dots[h])).astype(BF16)
-                dksend[l, :, c] = (dot_nn(g, q[:, c]) * scale).astype(BF16)
+                dsend[l, COMPACT : 2 * COMPACT, c] = (dot_nn(g, q[:, c]) * scale).astype(BF16)
                 dq[:, c] += dot_tn(g, kin[l, :, c])
             dk_copies[l].start()
 
@@ -247,12 +253,15 @@
         offer(l, jnp.logical_not(inside[l]) if l < 2 else True)
     for l in (1, 0):
         finish_level(l, near[l])
+    first = [me // 4 - (1 << l) // 4 == 0 for l in range(levels)]
+    for l in order[: levels - 2]:
+        finish_level(l, first[l])
     for l in landing:
 
         @pl.when(sends_up(l))
         def _(l=l):
             dv_copies[l].wait_recv()
-            dv[...] += dot_tn(pick[l], dvin[l])
+            dv[...] += dot_nn(pick[l], dvin[l])
 
     rounded = dv[...].astype(BF16)
     core = lax.rem(me, 2)
@@ -262,7 +271,8 @@
     pairs = quarter // 2
     mate = 2 * pair + 1 - odd
     chunk = 2 * rb
-    hr = rb // 2
+    pieces = send2.shape[1]
+    hr = rb // pieces
     others = quarter - 2
     turns, passes = [], []
     for t in range(others):
@@ -270,9 +280,6 @@
         above = jnp.where(there > pair, 1, 0)
         turns.append(2 * there + (t % 2) * (1 - above) + (1 - t % 2) * above)
         passes.append(above != odd)
-    def arrival(landed, sem, at, h):
-        return remote(landed.at[at, h], landed.at[at, h], sem.at[at, h], sem.at[at, h], flipped(1))
-
     s1, s2, p_copies, a_copies, b_copies = {}, {}, {}, {}, {}
 
     def share(t, at, side):
@@ -280,20 +287,20 @@
         w = dot_nn(xt[pl.ds(first, chunk), :], rounded)
         part[t] = w.reshape(2, rb, cols)
         s1[t] = remote(
-            part.at[t, 1 - core], got1.at[t], s1_ss.at[t], s1_rs.at[t], flipped(1)
+            part.at[t, 1 - core], got1.at[t], s1_ss, s1_rs.at[t], flipped(1)
         )
         s1[t].start()
 
     def halves():
-        return [(h, slice(h * hr, (h + 1) * hr)) for h in range(2)]
+        return [(h, slice(h * hr, (h + 1) * hr)) for h in range(pieces)]
 
     for t in range(quarter):
-        for h in range(2):
+        for h in range(pieces):
             s2[t, h] = remote(
-                send2.at[t, h], got2.at[t, h], s2_ss.at[t, h], s2_rs.at[t, h], flipped(2)
+                send2.at[t, h], got2.at[t, h], s2_ss.at[t], s2_rs.at[t, h], flipped(2)
             )
     for i in range(2):
-        p_copies[i] = remote(psend.at[i], pgot.at[i], p_ss.at[i], p_rs.at[i], tower(mate))
+        p_copies[i] = remote(psend.at[i], pgot.at[i], p_ss, p_rs.at[i], tower(mate))
 
     def cross(t, extra=None):
         s1[t].wait_recv()
@@ -316,34 +323,35 @@
             kept = part[quarter + t, core, span, :] + got1[quarter + t, span, :]
             kept = kept + got2[t, h].astype(F32)
             a_copies[t, h] = remote(
-                asend.at[t, h], agot.at[at, h], a_ss.at[t, h], a_rs.at[at, h], tower(mate)
+                zsend.at[t, h], agot.at[t, h], z_ss.at[t], a_rs.at[t, h], tower(mate)
             )
             b_copies[t, h] = remote(
-                bsend.at[t, h], bgot.at[high, h], b_ss.at[t, h], b_rs.at[high, h], tower(at)
+                zsend.at[t, h], bgot.at[t // 2, h], z_ss.at[t], b_rs.at[t // 2, h], tower(at)
             )
 
             @pl.when(passes[t])
             def _(kept=kept):
-                asend[t, h] = kept.astype(BF16)
+                zsend[t, h] = kept.astype(BF16)
                 a_copies[t, h].start()
 
             @pl.when(jnp.logical_not(passes[t]))
             def _(kept=kept):
-                arrival(agot, a_rs, at, h).wait_recv()
-                bsend[t, h] = (kept + agot[at, h].astype(F32)).astype(BF16)
+                a_copies[t, h].wait_recv()
+                zsend[t, h] = (kept + agot[t, h].astype(F32)).astype(BF16)
                 b_copies[t, h].start()
 
     far, home = quarter - 1, 2 * quarter - 1
     sender = passes[0]
     joiner = jnp.logical_not(sender)
     eager = jnp.logical_and(joiner, odd == 1)
-    patient = jnp.logical_and(joiner, odd == 0)
+    gives = jnp.logical_not(eager)
+    takes = jnp.logical_not(jnp.logical_and(sender, odd == 0))
     out_copies = {
         h: remote(
-            bsend.at[others, h], bgot.at[high, h],
-            b_ss.at[others, h], b_rs.at[high, h], tower(mate),
-        )
-        for h in range(2)
+            zsend.at[others, h], bgot.at[pairs - 1, h],
+            z_ss.at[others], b_rs.at[pairs - 1, h], tower(mate),
+        )
+        for h in range(pieces)
     }
 
     def mate_out():
@@ -351,7 +359,7 @@
         for h, span in halves():
             s2[others, h].wait_recv()
             kept = part[home - 1, core, span, :] + got1[home - 1, span, :]
-            bsend[others, h] = (kept + got2[others, h].astype(F32)).astype(BF16)
+            zsend[others, h] = (kept + got2[others, h].astype(F32)).astype(BF16)
             out_copies[h].start()
 
     share(0, turns[0], 1 - up)
@@ -359,10 +367,10 @@
     share(home - 1, mate, up)
     for t in range(1, others):
         share(t, turns[t], 1 - up)
+    cross(0)
     pl.when(eager)(lambda: cross(others))
-    cross(0)
-
-    @pl.when(sender)
+
+    @pl.when(gives)
     def _():
         pack(0, others)
         p_copies[0].start()
@@ -370,28 +378,28 @@
 
     for t in range(1, others):
         cross(t)
-    pl.when(patient)(lambda: cross(others))
     for l in landing:
-        finish_level(l, jnp.logical_and(joiner, jnp.logical_not(near[l])) if l < 2 else joiner)
+        finish_level(l, jnp.logical_and(joiner, jnp.logical_not((near if l < 2 else first)[l])))
     share(far, high, 1 - up)
     for t in range(others):
         share(quarter + t, turns[t], up)
     share(home, high, up)
+    relay(0)
     pl.when(eager)(mate_out)
-    relay(0)
-    pl.when(sender)(lambda: cross(far))
-
-    @pl.when(joiner)
-    def _():
+    pl.when(jnp.logical_not(takes))(lambda: cross(far))
+
+    def cross_home():
         p_copies[0].wait_recv()
         cross(far, pgot.at[0])
 
-    pl.when(patient)(mate_out)
+    pl.when(joiner)(cross_home)
+
     for t in range(1, others):
         relay(t)
+    pl.when(jnp.logical_and(sender, takes))(cross_home)
     for l in landing:
-        finish_level(l, jnp.logical_and(sender, jnp.logical_not(near[l])) if l < 2 else sender)
-    pl.when(sender)(p_copies[1].start)
+        finish_level(l, jnp.logical_and(sender, jnp.logical_not((near if l < 2 else first)[l])))
+    pl.when(gives)(p_copies[1].start)
     emit(dq, dq_out, scale)
     emit(dv, dv_out, 1.0)
     dk[...] = dk[...] * scale
@@ -400,7 +408,7 @@
         @pl.when(sends_up(l))
         def _(l=l):
             dk_copies[l].wait_recv()
-            dk[...] += dot_tn(pick[l], dkin[l])
+            dk[...] += dot_nn(pick[l], dkin[l])
 
     emit(dk, dk_out, 1.0)
 
@@ -410,40 +418,36 @@
         total = part[home, core, span, :] + got1[home, span, :]
         wg[span, :] = total + got2[far, h].astype(F32)
 
-    @pl.when(joiner)
+    @pl.when(takes)
     def _():
         p_copies[1].wait_recv()
         wg[...] += pgot[1].astype(F32)
 
-    for src in range(quarter):
-        relays = jnp.where(src < high, src % 2, 1 - src % 2) == 1
-        relays = jnp.where(src == mate, passes[0], relays)
-
-        @pl.when(jnp.logical_and(src != high, relays))
-        def _(src=src):
-            for h, span in halves():
-                arrival(bgot, b_rs, src, h).wait_recv()
-                wg[span, :] += bgot[src, h].astype(F32)
+    def absorb(i):
+        for h, span in halves():
+            remote(
+                zsend.at[i, h], bgot.at[i, h], z_ss.at[i], b_rs.at[i, h], tower(mate)
+            ).wait_recv()
+            wg[span, :] += bgot[i, h].astype(F32)
+
+    pl.when(jnp.logical_not(takes))(lambda: absorb(pairs - 1))
+    for i in range(pairs - 1):
+        absorb(i)
 
     wg_out[...] = wg[...]
     for l in order:
-        for copies in (slot_copies, dv_copies, dk_copies):
-            pl.when(sends_down(l))(copies[l].wait_send)
-        for copies in (k_copies, v_copies):
-            pl.when(sends_up(l))(copies[l].wait_send)
-    for copy in s1.values():
-        copy.wait_send()
-    for (t, h), copy in s2.items():
-        if t == others:
-            pl.when(joiner)(copy.wait_send)
-        else:
-            copy.wait_send()
-    for i in range(2):
-        pl.when(sender)(p_copies[i].wait_send)
-        pl.when(joiner)(out_copies[i].wait_send)
-    for (t, h), copy in a_copies.items():
-        pl.when(passes[t])(copy.wait_send)
-        pl.when(jnp.logical_not(passes[t]))(b_copies[t, h].wait_send)
+        fed = remote(kvsend.at[l], kvsend.at[l], up_ss.at[l], k_rs.at[l], to(1 << l))
+        pl.when(sends_up(l))(fed.wait_send)
+        fed = remote(dsend.at[l], dsend.at[l], down_ss.at[l], dv_rs.at[l], to(-(1 << l)))
+        pl.when(sends_down(l))(fed.wait_send)
+    remote(part.at[:, 0], got1, s1_ss, s1_rs.at[0], flipped(1)).wait_send()
+    for t in range(quarter):
+        sent = remote(send2.at[t], got2.at[t], s2_ss.at[t], s2_rs.at[t, 0], flipped(2))
+        pl.when(eager if t == others else True)(sent.wait_send)
+    for t in range(others + 1):
+        sent = remote(zsend.at[t], zsend.at[t], z_ss.at[t], a_rs.at[0, 0], tower(mate))
+        pl.when(eager if t == others else True)(sent.wait_send)
+    pl.when(gives)(remote(psend, pgot, p_ss, p_rs.at[0], tower(mate)).wait_send)
 
 
 def finish(*refs):
@@ -465,6 +469,7 @@
     cols = heads * dh
     width = layer_input.shape[1]
     rb = width // n
+    pieces = min(PIECES, rb // 8)
     rows = (levels + 1 + 7) // 8 * 8
     hbm = pl.BlockSpec(memory_space=pltpu.HBM)
     vmem = pl.BlockSpec(memory_space=pltpu.VMEM)
@@ -490,30 +495,39 @@
             pltpu.VMEM((width, tok), BF16),
             pltpu.VMEM((rows, tok), F32),
             pltpu.VMEM((levels, rows, tok), F32),
-            pltpu.VMEM((levels, COMPACT, tok), BF16),
+            pltpu.VMEM((levels, tok, COMPACT), BF16),
         ]
-        + [level_buf] * 8
+        + [pltpu.VMEM((levels, 2, COMPACT, cols), BF16), level_buf, level_buf]
+        + [pltpu.VMEM((levels, 2 * COMPACT + 2 * rows * tok // cols, cols), BF16)]
+        + [level_buf] * 2
         + [
             pltpu.VMEM((levels, heads, COMPACT, tok), F32),
             pltpu.VMEM((n // 2, 2, rb, cols), F32),
             pltpu.VMEM((n // 2, rb, cols), F32),
-            pltpu.VMEM((quarter, 2, rb // 2, cols), BF16),
-            pltpu.VMEM((quarter, 2, rb // 2, cols), BF16),
+            pltpu.VMEM((quarter, pieces, rb // pieces, cols), BF16),
+            pltpu.VMEM((quarter, pieces, rb // pieces, cols), BF16),
             pltpu.VMEM((2, rb, cols), BF16),
             pltpu.VMEM((2, rb, cols), BF16),
-        ]
-        + [pltpu.VMEM((quarter, 2, rb // 2, cols), BF16)] * 4
-        + [
+            pltpu.VMEM((quarter - 1, pieces, rb // pieces, cols), BF16),
+            pltpu.VMEM((quarter - 2, pieces, rb // pieces, cols), BF16),
+            pltpu.VMEM((quarter // 2, pieces, rb // pieces, cols), BF16),
             sems,
             sems,
             sems,
             sems((5,)),
         ]
-        + [sems((levels,))] * 10
-        + [sems((n // 2,))] * 2
-        + [sems((quarter, 2))] * 2
-        + [sems((2,))] * 2
-        + [sems((quarter, 2))] * 4,
+        + [sems((levels,))] * 7
+        + [
+            sems,
+            sems((n // 2,)),
+            sems((quarter,)),
+            sems((quarter, pieces)),
+            sems,
+            sems((2,)),
+            sems((quarter - 1,)),
+            sems((quarter - 2, pieces)),
+            sems((quarter // 2, pieces)),
+        ],
         compiler_params=pltpu.CompilerParams(
             collective_id=0, has_side_effects=True
         ),

time: 37.7 us -> 36.8 us (0.976)
  the two profiles are of different devices: /device:TPU:18 before, /device:TPU:0 now
where the time goes in v3:
time: 36.8 us; the launch traced here: 36.6 us
  Pallas kernels  36 us (98%)
  between operations  0.64 us (2%)
    pallas_call x1, Pallas kernels, per_device(): pl.pallas_call(functools.partial(body, n, levels, heads, dh), out_shape=[...  35 us
    pallas_call x1, Pallas kernels, per_device(): pl.pallas_call(finish, out_shape=[jax.ShapeDtypeStruct(o.shape, F32) for...  1 us

profile of v3, /device:TPU:0, one launch (start us, length us, event | category | flops | bytes accessed | tf_op | source)
XLA Modules:
  0.0 36.6 jit_solution(14317087751704437483)
XLA Ops:
  0.6 35.0 %shard_map.111 = (f32[512,128]{1,0:T(8,128)S(1)}, f32[512,128]{1,0:T(8,128)S(1)}, f32[512,128]{1,0:T(8,128)S(1)}, f32[256,256]{1,0:T(8,128)S(1)}) custom-call(s32[2,16]{1,0:T(2,128)} %picked_hbm.1, bf16[256,2,128]{2,1,0:T(2,128)(2,1)} %q_hbm.1, bf16[256,2,128]{2,1,0:T(2,128)(2,1)} %k_hbm.1, bf16[256,2,128]{2,1,0:T(2,128)(2,1)} %v_hbm.1, ...), custom_call_target="tpu_custom_call" | custom-call | tf_op jit(solution)/shard_map/pallas_call | solution.py:478
  35.6 1.0 %shard_map.112 = (f32[512,128]{1,0:T(8,128)}, f32[512,128]{1,0:T(8,128)}, f32[512,128]{1,0:T(8,128)}, f32[256,256]{1,0:T(8,128)}) custom-call(f32[512,128]{1,0:T(8,128)S(1)} %get-tuple-element.12.refs_0_, f32[512,128]{1,0:T(8,128)S(1)} %get-tuple-element.13.refs_1_, f32[512,128]{1,0:T(8,128)S(1)} %get-tuple-element.14.refs_2_, ...), custom_call_target="tpu_custom_call" | custom-call | tf_op jit(solution)/shard_map/pallas_call | solution.py:535

commit v4 on v3

--- a/solution.py
+++ b/solution.py
@@ -40,8 +40,8 @@
 def body(
     n, levels, heads, dh,
     picked_hbm, q_hbm, k_hbm, v_hbm, att_hbm, og_hbm, log_hbm, x_hbm,
-    dq_out, dk_out, dv_out, wg_out,
-    picked, log_sum, dq, dk, dv, wg, raw, q, k, v, att, og, x, xt, slot, slot_in, pick, kvsend, kin, vin, dsend, dvin, dkin,
+    dq_out, dk_out, dv_out, wg,
+    picked, log_sum, dq, dk, dv, raw, q, k, v, att, og, x, xt, slot, slot_in, pick, kvsend, kin, vin, dsend, dvin, dkin,
     wts, part, got1, send2, got2, psend, pgot, zsend, agot, bgot,
     x_sem, picked_sem, log_sem, raw_sem, up_ss, down_ss, slot_rs, k_rs, v_rs, dv_rs, dk_rs,
     s1_ss, s1_rs, s2_ss, s2_rs, p_ss, p_rs, z_ss, a_rs, b_rs,
@@ -53,7 +53,7 @@
     rows = slot.shape[0]
     scale = dh ** (-0.5)
     quarter = n // 4
-    rb = wg_out.shape[0]
+    rb = wg.shape[0]
     top = levels - 1
     order = list(reversed(range(levels)))
     landing = order
@@ -253,7 +253,12 @@
         offer(l, jnp.logical_not(inside[l]) if l < 2 else True)
     for l in (1, 0):
         finish_level(l, near[l])
-    first = [me // 4 - (1 << l) // 4 == 0 for l in range(levels)]
+    first = [
+        jnp.logical_and(
+            me // 4 == (1 << l) // 4, spot >= 2 if l == top else True
+        )
+        for l in range(levels)
+    ]
     for l in order[: levels - 2]:
         finish_level(l, first[l])
     for l in landing:
@@ -300,7 +305,7 @@
                 send2.at[t, h], got2.at[t, h], s2_ss.at[t], s2_rs.at[t, h], flipped(2)
             )
     for i in range(2):
-        p_copies[i] = remote(psend.at[i], pgot.at[i], p_ss, p_rs.at[i], tower(mate))
+        p_copies[i] = remote(psend.at[i], pgot.at[i], p_ss.at[i], p_rs.at[i], tower(mate))
 
     def cross(t, extra=None):
         s1[t].wait_recv()
@@ -344,37 +349,39 @@
     sender = passes[0]
     joiner = jnp.logical_not(sender)
     eager = jnp.logical_and(joiner, odd == 1)
-    gives = jnp.logical_not(eager)
-    takes = jnp.logical_not(jnp.logical_and(sender, odd == 0))
-    out_copies = {
-        h: remote(
-            zsend.at[others, h], bgot.at[pairs - 1, h],
-            z_ss.at[others], b_rs.at[pairs - 1, h], tower(mate),
-        )
-        for h in range(pieces)
-    }
+    hands = jnp.logical_and(eager, up == 0)
+    waits = jnp.logical_and(eager, up == 1)
+    gives = jnp.logical_not(hands)
+    outer = jnp.logical_and(sender, odd == 0)
+    takes = jnp.logical_not(jnp.logical_and(outer, up == 0))
 
     def mate_out():
         s1[home - 1].wait_recv()
         for h, span in halves():
             s2[others, h].wait_recv()
             kept = part[home - 1, core, span, :] + got1[home - 1, span, :]
-            zsend[others, h] = (kept + got2[others, h].astype(F32)).astype(BF16)
-            out_copies[h].start()
+            psend[1, span, :] = (kept + got2[others, h].astype(F32)).astype(BF16)
+        p_copies[1].start()
 
     share(0, turns[0], 1 - up)
     share(others, mate, 1 - up)
     share(home - 1, mate, up)
     for t in range(1, others):
         share(t, turns[t], 1 - up)
-    cross(0)
-    pl.when(eager)(lambda: cross(others))
-
-    @pl.when(gives)
-    def _():
+    def give():
         pack(0, others)
         p_copies[0].start()
+
+    pl.when(waits)(give)
+    cross(0)
+    pl.when(hands)(lambda: cross(others))
+    pl.when(jnp.logical_and(gives, jnp.logical_not(waits)))(give)
+
+    @pl.when(jnp.logical_not(waits))
+    def _():
         pack(1, home - 1)
+
+    pl.when(hands)(p_copies[1].start)
 
     for t in range(1, others):
         cross(t)
@@ -385,21 +392,21 @@
         share(quarter + t, turns[t], up)
     share(home, high, up)
     relay(0)
-    pl.when(eager)(mate_out)
+    pl.when(waits)(mate_out)
     pl.when(jnp.logical_not(takes))(lambda: cross(far))
 
     def cross_home():
         p_copies[0].wait_recv()
         cross(far, pgot.at[0])
 
-    pl.when(joiner)(cross_home)
+    pl.when(jnp.logical_and(takes, jnp.logical_or(joiner, odd == 0)))(cross_home)
 
     for t in range(1, others):
         relay(t)
-    pl.when(jnp.logical_and(sender, takes))(cross_home)
+    pl.when(jnp.logical_and(sender, odd == 1))(cross_home)
     for l in landing:
         finish_level(l, jnp.logical_and(sender, jnp.logical_not((near if l < 2 else first)[l])))
-    pl.when(gives)(p_copies[1].start)
+    pl.when(jnp.logical_not(eager))(p_copies[1].start)
     emit(dq, dq_out, scale)
     emit(dv, dv_out, 1.0)
     dk[...] = dk[...] * scale
@@ -418,11 +425,8 @@
         total = part[home, core, span, :] + got1[home, span, :]
         wg[span, :] = total + got2[far, h].astype(F32)
 
-    @pl.when(takes)
-    def _():
-        p_copies[1].wait_recv()
-        wg[...] += pgot[1].astype(F32)
-
+    p_copies[1].wait_recv()
+    wg[...] += pgot[1].astype(F32)
     def absorb(i):
         for h, span in halves():
             remote(
@@ -430,11 +434,9 @@
             ).wait_recv()
             wg[span, :] += bgot[i, h].astype(F32)
 
-    pl.when(jnp.logical_not(takes))(lambda: absorb(pairs - 1))
     for i in range(pairs - 1):
         absorb(i)
 
-    wg_out[...] = wg[...]
     for l in order:
         fed = remote(kvsend.at[l], kvsend.at[l], up_ss.at[l], k_rs.at[l], to(1 << l))
         pl.when(sends_up(l))(fed.wait_send)
@@ -443,11 +445,12 @@
     remote(part.at[:, 0], got1, s1_ss, s1_rs.at[0], flipped(1)).wait_send()
     for t in range(quarter):
         sent = remote(send2.at[t], got2.at[t], s2_ss.at[t], s2_rs.at[t, 0], flipped(2))
-        pl.when(eager if t == others else True)(sent.wait_send)
-    for t in range(others + 1):
+        pl.when(hands if t == others else True)(sent.wait_send)
+    for t in range(others):
         sent = remote(zsend.at[t], zsend.at[t], z_ss.at[t], a_rs.at[0, 0], tower(mate))
-        pl.when(eager if t == others else True)(sent.wait_send)
-    pl.when(gives)(remote(psend, pgot, p_ss, p_rs.at[0], tower(mate)).wait_send)
+        sent.wait_send()
+    pl.when(gives)(p_copies[0].wait_send)
+    p_copies[1].wait_send()
 
 
 def finish(*refs):
@@ -486,7 +489,6 @@
             pltpu.VMEM((tok, cols), F32),
             pltpu.VMEM((tok, cols), F32),
             pltpu.VMEM((tok, cols), F32),
-            pltpu.VMEM((rb, cols), F32),
             pltpu.VMEM((5, tok, heads, dh), BF16),
         ]
         + [pltpu.VMEM((tok, cols), BF16)] * 5
@@ -508,9 +510,9 @@
             pltpu.VMEM((quarter, pieces, rb // pieces, cols), BF16),
             pltpu.VMEM((2, rb, cols), BF16),
             pltpu.VMEM((2, rb, cols), BF16),
-            pltpu.VMEM((quarter - 1, pieces, rb // pieces, cols), BF16),
             pltpu.VMEM((quarter - 2, pieces, rb // pieces, cols), BF16),
-            pltpu.VMEM((quarter // 2, pieces, rb // pieces, cols), BF16),
+            pltpu.VMEM((quarter - 2, pieces, rb // pieces, cols), BF16),
+            pltpu.VMEM((quarter // 2 - 1, pieces, rb // pieces, cols), BF16),
             sems,
             sems,
             sems,
@@ -522,11 +524,11 @@
             sems((n // 2,)),
             sems((quarter,)),
             sems((quarter, pieces)),
-            sems,
             sems((2,)),
-            sems((quarter - 1,)),
+            sems((2,)),
+            sems((quarter - 2,)),
             sems((quarter - 2, pieces)),
-            sems((quarter // 2, pieces)),
+            sems((quarter // 2 - 1, pieces)),
         ],
         compiler_params=pltpu.CompilerParams(
             collective_id=0, has_side_effects=True

time: 36.8 us -> 36.7 us (level); the launches traced: 36.6 us -> 36 us
  Pallas kernels: 36 us -> 35.3 us
    pallas_call x1, Pallas kernels: 35 us -> 34.3 us  [per_device(): pl.pallas_call(functools.partial(body, n, levels, heads, dh), out_shape=[...]
where the time goes in v4:
time: 36.7 us; the launch traced here: 36 us
  Pallas kernels  35.3 us (96%)
  between operations  0.64 us (2%)
    pallas_call x1, Pallas kernels, per_device(): pl.pallas_call(functools.partial(body, n, levels, heads, dh), out_shape=[...  34.3 us
    pallas_call x1, Pallas kernels, per_device(): pl.pallas_call(finish, out_shape=[jax.ShapeDtypeStruct(o.shape, F32) for...  1 us

profile of v4, /device:TPU:0, one launch (start us, length us, event | category | flops | bytes accessed | tf_op | source)
XLA Modules:
  0.0 36.0 jit_solution(7939083043331392080)
XLA Ops:
  0.6 34.3 %shard_map.111 = (f32[512,128]{1,0:T(8,128)S(1)}, f32[512,128]{1,0:T(8,128)S(1)}, f32[512,128]{1,0:T(8,128)S(1)}, f32[256,256]{1,0:T(8,128)S(1)}) custom-call(s32[2,16]{1,0:T(2,128)} %picked_hbm.1, bf16[256,2,128]{2,1,0:T(2,128)(2,1)} %q_hbm.1, bf16[256,2,128]{2,1,0:T(2,128)(2,1)} %k_hbm.1, bf16[256,2,128]{2,1,0:T(2,128)(2,1)} %v_hbm.1, ...), custom_call_target="tpu_custom_call" | custom-call | tf_op jit(solution)/shard_map/pallas_call | solution.py:481
  35.0 1.0 %shard_map.112 = (f32[512,128]{1,0:T(8,128)}, f32[512,128]{1,0:T(8,128)}, f32[512,128]{1,0:T(8,128)}, f32[256,256]{1,0:T(8,128)}) custom-call(f32[512,128]{1,0:T(8,128)S(1)} %get-tuple-element.12.refs_0_, f32[512,128]{1,0:T(8,128)S(1)} %get-tuple-element.13.refs_1_, f32[512,128]{1,0:T(8,128)S(1)} %get-tuple-element.14.refs_2_, ...), custom_call_target="tpu_custom_call" | custom-call | tf_op jit(solution)/shard_map/pallas_call | solution.py:537

commit v5 on v4

--- a/solution.py
+++ b/solution.py
@@ -328,10 +328,10 @@
             kept = part[quarter + t, core, span, :] + got1[quarter + t, span, :]
             kept = kept + got2[t, h].astype(F32)
             a_copies[t, h] = remote(
-                zsend.at[t, h], agot.at[t, h], z_ss.at[t], a_rs.at[t, h], tower(mate)
+                zsend.at[t, h], agot.at[t, h], z_ss, a_rs.at[t, h], tower(mate)
             )
             b_copies[t, h] = remote(
-                zsend.at[t, h], bgot.at[t // 2, h], z_ss.at[t], b_rs.at[t // 2, h], tower(at)
+                zsend.at[t, h], bgot.at[t // 2, h], z_ss, b_rs.at[t // 2, h], tower(at)
             )
 
             @pl.when(passes[t])
@@ -430,7 +430,7 @@
     def absorb(i):
         for h, span in halves():
             remote(
-                zsend.at[i, h], bgot.at[i, h], z_ss.at[i], b_rs.at[i, h], tower(mate)
+                zsend.at[i, h], bgot.at[i, h], z_ss, b_rs.at[i, h], tower(mate)
             ).wait_recv()
             wg[span, :] += bgot[i, h].astype(F32)
 
@@ -446,9 +446,7 @@
     for t in range(quarter):
         sent = remote(send2.at[t], got2.at[t], s2_ss.at[t], s2_rs.at[t, 0], flipped(2))
         pl.when(hands if t == others else True)(sent.wait_send)
-    for t in range(others):
-        sent = remote(zsend.at[t], zsend.at[t], z_ss.at[t], a_rs.at[0, 0], tower(mate))
-        sent.wait_send()
+    remote(zsend, zsend, z_ss, a_rs.at[0, 0], tower(mate)).wait_send()
     pl.when(gives)(p_copies[0].wait_send)
     p_copies[1].wait_send()
 
@@ -526,7 +524,7 @@
             sems((quarter, pieces)),
             sems((2,)),
             sems((2,)),
-            sems((quarter - 2,)),
+            sems,
             sems((quarter - 2, pieces)),
             sems((quarter // 2 - 1, pieces)),
         ],

time: 36.7 us -> 36.7 us (level)
  no operation moved by 1% of the time
where the time goes in v5:
time: 36.7 us; the launch traced here: 36 us
  Pallas kernels  35.3 us (96%)
  between operations  0.64 us (2%)
    pallas_call x1, Pallas kernels, per_device(): pl.pallas_call(functools.partial(body, n, levels, heads, dh), out_shape=[...  34.3 us
    pallas_call x1, Pallas kernels, per_device(): pl.pallas_call(finish, out_shape=[jax.ShapeDtypeStruct(o.shape, F32) for...  1 us

profile of v5, /device:TPU:0, one launch (start us, length us, event | category | flops | bytes accessed | tf_op | source)
XLA Modules:
  0.0 36.0 jit_solution(14912464250083695826)
XLA Ops:
  0.6 34.3 %shard_map.111 = (f32[512,128]{1,0:T(8,128)S(1)}, f32[512,128]{1,0:T(8,128)S(1)}, f32[512,128]{1,0:T(8,128)S(1)}, f32[256,256]{1,0:T(8,128)S(1)}) custom-call(s32[2,16]{1,0:T(2,128)} %picked_hbm.1, bf16[256,2,128]{2,1,0:T(2,128)(2,1)} %q_hbm.1, bf16[256,2,128]{2,1,0:T(2,128)(2,1)} %k_hbm.1, bf16[256,2,128]{2,1,0:T(2,128)(2,1)} %v_hbm.1, ...), custom_call_target="tpu_custom_call" | custom-call | tf_op jit(solution)/shard_map/pallas_call | solution.py:479
  35.0 1.0 %shard_map.112 = (f32[512,128]{1,0:T(8,128)}, f32[512,128]{1,0:T(8,128)}, f32[512,128]{1,0:T(8,128)}, f32[256,256]{1,0:T(8,128)}) custom-call(f32[512,128]{1,0:T(8,128)S(1)} %get-tuple-element.12.refs_0_, f32[512,128]{1,0:T(8,128)S(1)} %get-tuple-element.13.refs_1_, f32[512,128]{1,0:T(8,128)S(1)} %get-tuple-element.14.refs_2_, ...), custom_call_target="tpu_custom_call" | custom-call | tf_op jit(solution)/shard_map/pallas_call | solution.py:535
